TPU v7x, 32 devices: a whole 2x2x4 slice. The times are simulated.
32 devices in a mesh: grp: 2 (over y), tp: 4 (over z), dp: 4 (over x, core).
Axes of the slice: x: 2, y: 2, z: 4, core: 2. Of those that a mesh axis runs over, the one named last changes fastest.
Arguments:
- tokens: bfloat16 [512, 4096], P('grp', 'dp'), parts along dimension 0, may hold values from -40 to 40
- sequence_lengths: int32 [512], P(('grp', 'dp')), parts along dimension 0, may hold values from 1 to 4096, 262144 in all
- recurrent_state: float32 [2, 512, 128, 128], P(None, ('grp', 'dp'), 'tp'), parts along dimension 1, may hold values from -1.8 to 1.8
- norm_weight: float32 [2, 4096], P(None, 'dp'), may hold values from 0.1 to 1.9
- input_weight: bfloat16 [2, 4096, 2048], P(None, 'dp', 'tp'), may hold values from -0.09375 to 0.09375
- gate_weight: bfloat16 [2, 4096, 2048], P(None, 'dp', 'tp'), may hold values from -0.09375 to 0.09375
- output_weight: bfloat16 [2, 2048, 4096], P(None, 'tp', 'dp'), may hold values from -0.125 to 0.125
- negated_real_rate: float32 [2, 8192], P(None, 'tp'), may hold values from 0.005 to 1
- frequency: float32 [2, 8192], P(None, 'tp'), may hold values from -4 to 4
- discrete_step: float32 [2, 128], P(None, 'tp'), may hold values from 0.02 to 0.5
- group_input_matrix: float32 [2, 128, 16, 128], P(None, 'tp'), may hold values from -1.5 to 1.5
- group_output_matrix: float32 [2, 128, 16, 128], P(None, 'tp'), may hold values from -0.5 to 0.5
- feedthrough_weight: float32 [2, 2048], P(None, 'tp'), may hold values from -3 to 3
- extra_log_decay: float32 [2, 128, 4096], P(None, 'tp'), may hold values from -0.7 to 0
Outputs:
- tokens_out: bfloat16 [512, 4096], P('grp', 'dp'), parts along dimension 0
- state_out: float32 [2, 512, 128, 128], P(None, ('grp', 'dp'), 'tp'), parts along dimension 1
There are 2 independent parts, one for each index of `grp`. A program takes and returns all parts, laid end to end along the dimension named above; an argument that names none is the same for every part. Nothing has to cross between parts.
Inputs may be any that keep to these rules, and one draw needn't show every extreme that they name: The newest token of a sequence stands at position sequence_lengths - 1.
All inputs are finite; a program needn't handle non-finite values. No bound on the sum of `sequence_lengths` on one device may be relied on, other than what follows from the above.
Results may differ from a plain program's by a relative error of at most 0.009.
Values may be sent and summed in bfloat16 or wider, within the bound.
A program may use at most 64 MiB of HBM per device.

v0:
```python
import jax
import jax.numpy as jnp
from jax import lax
from jax.sharding import PartitionSpec as P

D = 4096
STACKED_LAYERS = 2
TOP_PRECISION = lax.Precision.HIGHEST
NORM_EPS = 1e-06


def transition(decay_factor, angular_frequency, step_width):
    log_mag = -decay_factor * step_width[:, None]
    turn = angular_frequency * step_width[:, None]
    magnitude = jnp.exp(log_mag)
    discrete_real = magnitude * jnp.cos(turn)
    discrete_imaginary = magnitude * jnp.sin(turn)
    half_sine = jnp.sin(0.5 * turn)
    numer_re = jnp.expm1(log_mag) * jnp.cos(turn) - 2.0 * half_sine * half_sine
    denom = decay_factor * decay_factor + angular_frequency * angular_frequency
    drive_re = (-numer_re * decay_factor + discrete_imaginary * angular_frequency) / denom
    drive_im = (-discrete_imaginary * decay_factor - numer_re * angular_frequency) / denom
    return (discrete_real, discrete_imaginary, drive_re, drive_im)


def state_space_update(
    input_groups,
    layer_state,
    extra_decay_factor,
    decay_factor,
    angular_frequency,
    step_width,
    input_matrix,
    readout_matrix,
):
    half_width = input_matrix.shape[-1] // 2
    decay_factor = decay_factor.reshape(-1, half_width)
    angular_frequency = angular_frequency.reshape(-1, half_width)
    discrete_real, discrete_imaginary, drive_re, drive_im = transition(
        decay_factor, angular_frequency, step_width
    )
    input_real = input_matrix[..., :half_width]
    input_imaginary = input_matrix[..., half_width:]
    driven_input_real = jnp.einsum(
        "tkl,klf->tkf", input_groups, input_real, precision=TOP_PRECISION
    )
    driven_input_imaginary = jnp.einsum(
        "tkl,klf->tkf", input_groups, input_imaginary, precision=TOP_PRECISION
    )
    state_re = layer_state[..., :half_width]
    state_im = layer_state[..., half_width:]
    carried_real = extra_decay_factor[..., None] * discrete_real[None]
    carried_imaginary = extra_decay_factor[..., None] * discrete_imaginary[None]
    updated_real = (
        carried_real * state_re
        - carried_imaginary * state_im
        + drive_re[None] * driven_input_real
        - drive_im[None] * driven_input_imaginary
    )
    updated_imaginary = (
        carried_real * state_im
        + carried_imaginary * state_re
        + drive_re[None] * driven_input_imaginary
        + drive_im[None] * driven_input_real
    )
    readout_rows = jnp.einsum(
        "hzk,dhk->dhz", readout_matrix[..., :half_width], updated_real, precision=TOP_PRECISION
    ) - jnp.einsum(
        "hzk,dhk->dhz", readout_matrix[..., half_width:], updated_imaginary, precision=TOP_PRECISION
    )
    return (readout_rows, jnp.concatenate([updated_real, updated_imaginary], axis=-1))


def single_layer(
    hidden_rows,
    sequence_lengths,
    layer_state,
    norm_scale_rows,
    input_matrix_weight,
    gate_matrix,
    output_matrix_weight,
    decay_factor,
    angular_frequency,
    step_width,
    input_matrix,
    readout_matrix,
    feedthrough_rows,
    extra_decay_rows,
):
    x_float = hidden_rows.astype(jnp.float32)
    square_sums = jnp.sum(x_float * x_float, axis=1)
    scaled_in = (x_float * norm_scale_rows[None, :]).astype(jnp.bfloat16)
    input_part = jnp.dot(scaled_in, input_matrix_weight, preferred_element_type=jnp.float32)
    gate_part = jnp.dot(scaled_in, gate_matrix, preferred_element_type=jnp.float32)
    local_rows = sequence_lengths.shape[0]
    input_sum, gate_sum, mine_squares = (
        lax.psum_scatter(input_part, "dp", scatter_dimension=0, tiled=True),
        lax.psum_scatter(gate_part, "dp", scatter_dimension=0, tiled=True),
        lax.psum_scatter(square_sums, "dp", scatter_dimension=0, tiled=True),
    )
    scale = lax.rsqrt(mine_squares / D + NORM_EPS)[:, None]
    u_vals = (input_sum * scale).astype(jnp.bfloat16)
    gate_vals = (gate_sum * scale).astype(jnp.bfloat16)
    group_count = layer_state.shape[1]
    input_float = u_vals.astype(jnp.float32)
    token_positions = sequence_lengths - 1
    extra_decay_factor = jnp.exp(jnp.take(extra_decay_rows, token_positions, axis=1).T)
    readout_rows, updated_state = state_space_update(
        input_float.reshape(local_rows, group_count, -1),
        layer_state,
        extra_decay_factor,
        decay_factor,
        angular_frequency,
        step_width,
        input_matrix,
        readout_matrix,
    )
    y_vals = jax.nn.gelu(
        readout_rows.reshape(local_rows, -1) + feedthrough_rows[None, :] * input_float
    )
    mixed = (y_vals * jax.nn.sigmoid(gate_vals.astype(jnp.float32))).astype(jnp.bfloat16)
    branch_terms = jnp.dot(
        lax.all_gather(mixed, "dp", axis=0, tiled=True),
        output_matrix_weight,
        preferred_element_type=jnp.float32,
    )
    branch = lax.psum(branch_terms, "tp").astype(jnp.bfloat16)
    x_next = (x_float + branch.astype(jnp.float32)).astype(jnp.bfloat16)
    return (x_next, updated_state)


def on_device(
    tokens,
    sequence_lengths,
    recurrent_state,
    norm_weight,
    input_weight,
    gate_weight,
    output_weight,
    negated_real_rate,
    frequency,
    discrete_step,
    group_input_matrix,
    group_output_matrix,
    feedthrough_weight,
    extra_log_decay,
):
    hidden_rows = tokens
    states = []
    for index_of_layer in range(STACKED_LAYERS):
        hidden_rows, updated_state = single_layer(
            hidden_rows,
            sequence_lengths,
            recurrent_state[index_of_layer],
            norm_weight[index_of_layer],
            input_weight[index_of_layer],
            gate_weight[index_of_layer],
            output_weight[index_of_layer],
            negated_real_rate[index_of_layer],
            frequency[index_of_layer],
            discrete_step[index_of_layer],
            group_input_matrix[index_of_layer],
            group_output_matrix[index_of_layer],
            feedthrough_weight[index_of_layer],
            extra_log_decay[index_of_layer],
        )
        states.append(updated_state)
    return (hidden_rows, jnp.stack(states, axis=0))


def solution(mesh):
    in_specs = (
        P("grp", "dp"),
        P(("grp", "dp")),
        P(None, ("grp", "dp"), "tp", None),
        P(None, "dp"),
        P(None, "dp", "tp"),
        P(None, "dp", "tp"),
        P(None, "tp", "dp"),
        P(None, "tp"),
        P(None, "tp"),
        P(None, "tp"),
        P(None, "tp", None, None),
        P(None, "tp", None, None),
        P(None, "tp"),
        P(None, "tp", None),
    )
    out_specs = (P("grp", "dp"), P(None, ("grp", "dp"), "tp", None))
    return jax.shard_map(
        on_device, mesh=mesh, in_specs=in_specs, out_specs=out_specs, check_vma=False
    )
```

profile of v0, /device:TPU:0, one launch (start us, length us, event | category | flops | bytes accessed | tf_op | source)
XLA Modules:
  0.0 220.6 jit_solution(5358436251447161086)
XLA Ops:
  7.2 0.8 fusion.85
  8.0 2.6 %fusion.28 = f32[256,512]{1,0:T(8,128)} fusion(bf16[2,1024,512]{2,1,0:T(8,128)(2,1)} %param.20, bf16[256,1024]{1,0:T(8,128)(2,1)} %param.16, f32[1024]{0:T(1024)S(1)} %bitcast.103), kind=kOutput, calls=%fused_computation.51 | convolution fusion | flops 269221888 | bytes 2101248 | tf_op jit(solution)/shard_map/dot_general | solution.py:93
  10.7 0.0 reduce-scatter.7.cloned.1.call-start
  10.8 2.6 %fusion.26 = f32[256,512]{1,0:T(8,128)} fusion(bf16[2,1024,512]{2,1,0:T(8,128)(2,1)} %param.21, bf16[256,1024]{1,0:T(8,128)(2,1)S(1)} %copy-done.3, f32[1024]{0:T(1024)S(1)} %bitcast.104), kind=kOutput, calls=%fused_computation.49 | convolution fusion | flops 269221888 | bytes 2101248 | tf_op jit(solution)/shard_map/dot_general | solution.py:94
  13.4 0.2 fusion.13
  13.6 8.5 %all-reduce = f32[256]{0:T(256)S(1)} all-reduce(f32[256]{0:T(256)S(1)} %fusion.13), channel_id=3, replica_groups=mesh['grp'=2,'tp'=4,'dp'=4] {'dp'}, use_global_device_ids=true, to_apply=%region_2.4.clone | all-reduce | flops 256 | bytes 2048
  22.2 0.1 slice_reduce_fusion
  22.3 0.1 reshape_squeeze.13
  22.4 0.1 reshape_squeeze.12
  22.5 0.7 slice_bitcast_fusion.1
  23.2 0.9 fusion.84
  24.1 1.6 copy.53
  25.8 1.9 copy.51
  27.7 0.6 gather_fusion.1
  28.3 2.3 %gather_fusion = f32[64,32]{1,0:T(8,128)S(1)} fusion(f32[32,4096]{0,1:T(8,128)} %bitcast.92, s32[1024]{0:T(1024)S(1)} %pad_clamp_fusion), kind=kCustom, calls=%fused_computation.clone | custom fusion | bytes 16640 | tf_op jit(solution)/shard_map/jit(_take)/gather | solution.py:107
  30.5 0.1 fusion.72
  30.6 0.1 copy.41
  30.7 1.7 fusion.83
  32.5 0.6 dynamic-slice
  33.7 0.1 fusion.80
  33.8 2.5 %copy_bitcast_fusion = (f32[64,32,128]{2,0,1:T(8,128)}, f32[64,32,128]{2,0,1:T(8,128)}) fusion(f32[1,64,32,128]{3,2,1,0:T(8,128)S(1)} %get-tuple-element.21, f32[1,64,32,128]{3,2,1,0:T(8,128)S(1)} %get-tuple-element.22), kind=kLoop, calls=%fused_computation.39 | loop fusion | bytes 4194304 | tf_op jit(solution)/shard_map/squeeze | solution.py:154
  36.3 0.2 exponential_multiply_fusion.1
  36.5 1.0 multiply_convert_fusion.3
  37.5 0.1 copy.43
  37.7 0.8 fusion.50
  38.5 2.8 %fusion.5 = (f32[64,32,64]{2,0,1:T(8,128)S(1)}, f32[64,32,64]{2,0,1:T(8,128)S(1)}) fusion(f32[32,64,64]{2,1,0:T(8,128)S(1)} %fusion.50, f32[64,32,128]{2,0,1:T(8,128)} %get-tuple-element.46, f32[32,64]{1,0:T(8,128)S(1)} %get-tuple-element.36, f32[32,64]{1,0:T(8,128)S(1)} %get-tuple-element.35, f32[32,64]{1,0:T(8,128)S(1)} %get-tuple-element.34, ...), kind=kOutput, calls=%fused_computation.24 | convolution fusion | flops 27262976 | bytes 2990080 | tf_op jit(solution)/shard_map/tkl,klf->tkf/dot_general | solution.py:44
  41.3 1.7 fusion.48
  43.0 1.8 convolution_subtract_fusion.1
  44.8 0.1 copy.44
  45.0 14.7 %reduce-scatter.7.cloned.1.call-done = f32[64,512]{1,0:T(8,128)} async-done(((f32[256,512]{1,0:T(8,128)}), f32[64,512]{1,0:T(8,128)}) %reduce-scatter.7.cloned.1.call-update) | async-done | bytes 131088 | tf_op jit(solution)/shard_map/reduce_scatter | solution.py:98
  59.6 1.1 fusion.62
  60.7 5.8 %all_gather.6 = bf16[256,512]{1,0:T(8,128)(2,1)S(1)} all-gather(bf16[64,512]{1,0:T(8,128)(2,1)S(1)} %fusion.62), channel_id=1, replica_groups=mesh['grp'=2,'tp'=4,'dp'=4] {'dp'}, dimensions={0}, use_global_device_ids=true | all-gather | bytes 327680 | tf_op jit(solution)/shard_map/all_gather | solution.py:123
  66.5 1.7 fusion.24
  68.1 44.3 %all-reduce.4 = bf16[256,1024]{1,0:T(8,128)(2,1)} all-reduce(f32[256,1024]{1,0:T(8,128)S(1)} %fusion.24), channel_id=1, replica_groups=mesh['grp'=2,'tp'=4,'dp'=4] {'tp'}, use_global_device_ids=true, to_apply=%region_4.0 | all-reduce | flops 262144 | bytes 1572864 | tf_op jit(solution)/shard_map/psum | solution.py:127
  112.4 1.5 fusion.16
  113.9 2.7 %fusion.22 = f32[256,512]{1,0:T(8,128)} fusion(bf16[2,1024,512]{2,1,0:T(8,128)(2,1)} %param.20, bf16[256,1024]{1,0:T(8,128)(2,1)S(1)} %get-tuple-element.14, f32[1024]{0:T(1024)S(1)} %bitcast.101), kind=kOutput, calls=%fused_computation.45 | convolution fusion | flops 269221888 | bytes 2101248 | tf_op jit(solution)/shard_map/dot_general | solution.py:93
  116.6 0.0 reduce-scatter.11.cloned.1.call-start
  116.6 0.1 reshape_squeeze.15
  116.7 0.1 reshape_squeeze.14
  116.8 0.1 copy.46
  116.8 0.2 exponential_multiply_fusion
  117.1 6.2 %all-reduce.1 = f32[256]{0:T(256)S(1)} all-reduce(f32[256]{0:T(256)S(1)} %get-tuple-element.13), channel_id=6, replica_groups=mesh['grp'=2,'tp'=4,'dp'=4] {'dp'}, use_global_device_ids=true, to_apply=%region_7.9.clone | all-reduce | flops 256 | bytes 2048
  123.2 0.1 fusion.81
  123.3 0.3 maximum_bitcast_fusion
  123.6 1.2 copy-done.15
  124.8 0.1 copy-done.2
  124.9 1.2 fusion.20
  126.2 10.6 %reduce-scatter.9.cloned.1.call-done = f32[64,512]{1,0:T(8,128)} async-done(((f32[256,512]{1,0:T(8,128)}), f32[64,512]{1,0:T(8,128)}) %reduce-scatter.9.cloned.1.call-update) | async-done | bytes 131088 | tf_op jit(solution)/shard_map/reduce_scatter | solution.py:97
  136.8 1.0 multiply_convert_fusion.1
  137.8 0.1 copy.48
  137.9 0.8 fusion.43
  138.7 1.5 fusion.11
  140.2 0.3 maximum_bitcast_fusion.1
  140.5 0.2 pad_maximum_fusion
  140.8 2.5 %copy.50 = f32[2,64,32,128]{3,2,1,0:T(8,128)} copy(f32[2,64,32,128]{3,1,2,0:T(8,128)S(1)} %pad_maximum_fusion) | data formatting | bytes 4194304
  143.3 1.7 fusion.41
  145.0 1.8 convolution_subtract_fusion
  146.9 0.1 copy.49
  147.0 13.8 %reduce-scatter.11.cloned.1.call-done = f32[64,512]{1,0:T(8,128)} async-done(((f32[256,512]{1,0:T(8,128)}), f32[64,512]{1,0:T(8,128)}) %reduce-scatter.11.cloned.1.call-update) | async-done | bytes 131088 | tf_op jit(solution)/shard_map/reduce_scatter | solution.py:98
  160.8 1.1 fusion.71
  161.9 5.8 %all_gather.7 = bf16[256,512]{1,0:T(8,128)(2,1)S(1)} all-gather(bf16[64,512]{1,0:T(8,128)(2,1)S(1)} %fusion.71), channel_id=1, replica_groups=mesh['grp'=2,'tp'=4,'dp'=4] {'dp'}, dimensions={0}, use_global_device_ids=true | all-gather | bytes 327680 | tf_op jit(solution)/shard_map/all_gather | solution.py:123
  167.7 0.4 fusion.18
  168.1 43.9 %all-reduce.5 = bf16[256,1024]{1,0:T(8,128)(2,1)S(1)} all-reduce(f32[256,1024]{1,0:T(8,128)S(1)} %fusion.18), channel_id=1, replica_groups=mesh['grp'=2,'tp'=4,'dp'=4] {'tp'}, use_global_device_ids=true, to_apply=%region_9.11 | all-reduce | flops 262144 | bytes 1572864 | tf_op jit(solution)/shard_map/psum | solution.py:127
  212.0 2.0 fusion.17
  (46 shorter events, 0.3 us)
Async XLA Ops:
  7.2 3.6 %copy-start.3 = (bf16[256,1024]{1,0:T(8,128)(2,1)S(1)}, bf16[256,1024]{1,0:T(8,128)(2,1)}, u32[]{:S(2)}) copy-start(bf16[256,1024]{1,0:T(8,128)(2,1)} %param.16) | copy-start | bytes 1572868
  7.2 29.4 %reduce-scatter.5.cloned.1.call-start = ((), (), s32[]{:S(2)}) async-start(), calls=%async_computation.4 | async-start | bytes 655360 | tf_op jit(solution)/shard_map/reduce_scatter | solution.py:97
  10.6 11.5 %copy-start.16 = (s32[64]{0:T(128)S(1)}, s32[64]{0:T(128)}, u32[]{:S(2)}) copy-start(s32[64]{0:T(128)} %param.17) | copy-start | bytes 772
  10.6 11.5 %copy-start.14 = (f32[2,32]{1,0:T(2,128)S(1)}, f32[2,32]{1,0:T(2,128)}, u32[]{:S(2)}) copy-start(f32[2,32]{1,0:T(2,128)} %param.25) | copy-start | bytes 772
  10.6 11.5 %copy-start.13 = (f32[2,512]{1,0:T(2,128)S(1)}, f32[2,512]{1,0:T(2,128)}, u32[]{:S(2)}) copy-start(f32[2,512]{1,0:T(2,128)} %param.28) | copy-start | bytes 12292
  10.6 11.6 %copy-start.11 = (f32[2,2048]{1,0:T(2,128)S(1)}, f32[2,2048]{1,0:T(2,128)}, u32[]{:S(2)}) copy-start(f32[2,2048]{1,0:T(2,128)} %param.24) | copy-start | bytes 49156
  10.7 11.6 %copy-start.12 = (f32[2,2048]{1,0:T(2,128)S(1)}, f32[2,2048]{1,0:T(2,128)}, u32[]{:S(2)}) copy-start(f32[2,2048]{1,0:T(2,128)} %param.23) | copy-start | bytes 49156
  10.7 11.8 %copy-start.7 = (f32[2,32,16,128]{3,2,1,0:T(8,128)S(1)}, f32[2,32,16,128]{3,2,1,0:T(8,128)}, u32[]{:S(2)}) copy-start(f32[2,32,16,128]{3,2,1,0:T(8,128)} %param.26) | copy-start | bytes 1572868
  10.7 12.5 %copy-start.8 = (f32[2,32,16,128]{3,2,1,0:T(8,128)S(1)}, f32[2,32,16,128]{3,2,1,0:T(8,128)}, u32[]{:S(2)}) copy-start(f32[2,32,16,128]{3,2,1,0:T(8,128)} %param.27) | copy-start | bytes 1572868
  10.7 48.9 %reduce-scatter.7.cloned.1.call-start = ((), (), s32[]{:S(2)}) async-start(), calls=%async_computation.5 | async-start | bytes 655360 | tf_op jit(solution)/shard_map/reduce_scatter | solution.py:98
  13.4 9.9 %copy-start.4 = (f32[2,32,4096]{2,1,0:T(8,128)S(1)}, f32[2,32,4096]{2,1,0:T(8,128)}, u32[]{:S(2)}) copy-start(f32[2,32,4096]{2,1,0:T(8,128)} %param.29) | copy-start | bytes 3145732
  13.4 123.4 %reduce-scatter.9.cloned.1.call-start = ((), (), s32[]{:S(2)}) async-start(), calls=%async_computation.6 | async-start | bytes 655360 | tf_op jit(solution)/shard_map/reduce_scatter | solution.py:97
  30.7 1.8 copy-start.17
  41.3 18.3 %copy-start.9 = (f32[64,512]{1,0:T(8,128)S(1)}, f32[64,512]{1,0:T(8,128)}, u32[]{:S(2)}) copy-start(f32[64,512]{1,0:T(8,128)} %reduce-scatter.5.cloned.1.call-done) | copy-start | bytes 393220
  113.9 9.3 %copy-start.1 = (bf16[256,1024]{1,0:T(8,128)(2,1)}, bf16[256,1024]{1,0:T(8,128)(2,1)S(1)}, u32[]{:S(2)}) copy-start(bf16[256,1024]{1,0:T(8,128)(2,1)S(1)} %get-tuple-element.14) | copy-start | bytes 1572868
  116.6 44.2 %reduce-scatter.11.cloned.1.call-start = ((), (), s32[]{:S(2)}) async-start(), calls=%async_computation.7 | async-start | bytes 655360 | tf_op jit(solution)/shard_map/reduce_scatter | solution.py:98
  123.2 1.6 copy-start.15
  123.3 1.6 copy-start.2
  124.9 13.0 %copy-start.6 = (f32[32,16,128]{2,1,0:T(8,128)S(1)}, f32[32,16,128]{2,1,0:T(8,128)}, u32[]{:S(2)}) copy-start(f32[32,16,128]{2,1,0:T(8,128)} %get-tuple-element.27) | copy-start | bytes 786436
  124.9 13.8 %copy-start.5 = (f32[64,32,128]{2,0,1:T(8,128)S(1)}, f32[64,32,128]{2,0,1:T(8,128)}, u32[]{:S(2)}) copy-start(f32[64,32,128]{2,0,1:T(8,128)} %get-tuple-element.45) | copy-start | bytes 3145732
  143.3 17.5 %copy-start.10 = (f32[64,512]{1,0:T(8,128)S(1)}, f32[64,512]{1,0:T(8,128)}, u32[]{:S(2)}) copy-start(f32[64,512]{1,0:T(8,128)} %reduce-scatter.9.cloned.1.call-done) | copy-start | bytes 393220
  143.3 24.3 %copy-start = (bf16[2,512,1024]{2,1,0:T(8,128)(2,1)S(1)}, bf16[2,512,1024]{2,1,0:T(8,128)(2,1)}, u32[]{:S(2)}) copy-start(bf16[2,512,1024]{2,1,0:T(8,128)(2,1)} %param.22) | copy-start | bytes 6291460
Sparse Core Ops, SparseCore 0:
  11.0 24.3 reduce-scatter.4
  38.0 21.6 reduce-scatter.6
  116.7 20.0 reduce-scatter.8
  139.1 21.6 reduce-scatter.10
where the time goes:
time: 221 us
  blocking collectives  114 us (52%)
  waiting for transfers between devices  39.2 us (18%)
  matrix products  24.2 us (11%)
  local copies, waits for them, and re-layouts  18.5 us (8%)
  between operations  14.8 us (7%)
  other arithmetic  9.38 us (4%)
    psum x2, blocking collectives, single_layer(): branch = lax.psum(branch_terms, 'tp').astype(jnp.bfloat16)  88.2 us
    reduce_scatter x2, waiting for transfers between devices, single_layer(): lax.psum_scatter(gate_part, 'dp', scatter_dimension=0, tiled=True)  28.5 us
    unnamed x2, blocking collectives  14.7 us
    all_gather x2, blocking collectives, single_layer(): lax.all_gather(mixed, 'dp', axis=0, tiled=True)  11.6 us
    reduce_scatter x2, waiting for transfers between devices, single_layer(): lax.psum_scatter(input_part, 'dp', scatter_dimension=0, tiled=True)  10.6 us
    unnamed x40, local copies, waits for them, and re-layouts  8.03 us
    dot_general x2, matrix products, single_layer(): jnp.dot(scaled_in, input_matrix_weight, preferred_element_type=jnp.float32)  5.28 us
  transfers between devices with their start and end apart: 4, of which 3 were waited for; matrix products, arithmetic and copies ran while one was open for 17% of the time, Pallas kernels for 0%

commit v1 on v0

--- a/solution.py
+++ b/solution.py
@@ -124,7 +124,7 @@
         output_matrix_weight,
         preferred_element_type=jnp.float32,
     )
-    branch = lax.psum(branch_terms, "tp").astype(jnp.bfloat16)
+    branch = jnp.sum(lax.all_gather(branch_terms, "tp"), axis=0).astype(jnp.bfloat16)
     x_next = (x_float + branch.astype(jnp.float32)).astype(jnp.bfloat16)
     return (x_next, updated_state)
 

time: 221 us -> 303 us (1.37)
  waiting for transfers between devices: 39.2 us -> 194 us
  blocking collectives: 114 us -> 26.5 us
  matrix products: 24.2 us -> 30.7 us
  other arithmetic: 9.38 us -> 14.2 us
    all_gather x0 -> x2, waiting for transfers between devices: none -> 157 us  [single_layer(): lax.all_gather(branch_terms, 'tp')]
    psum x2 -> x0, blocking collectives: 88.2 us -> none  [single_layer(): branch = lax.psum(branch_terms, 'tp').astype(jnp.bfloat16)]
    reduce_sum x0 -> x2, other arithmetic: none -> 5.44 us  [single_layer(): jnp.sum(lax.all_gather(branch_terms, 'tp'), axis=0).astype(jnp.bfloat16)]
    dot_general x2, matrix products: 2.09 us -> 5.26 us  [single_layer(): jnp.dot(lax.all_gather(mixed, 'dp', axis=0, tiled=True), output_matrix_we...]
    unnamed x40 -> x44, local copies, waits for them, and re-layouts: 8.03 us -> 8.59 us
  transfers between devices with their start and end apart: 4 -> 6, of which waited for: 3 -> 5; matrix products, arithmetic and copies ran while one was open for 17% -> 14% of each run, Pallas kernels for 0% -> 0%
where the time goes in v1:
time: 303 us; the launch traced here: 302 us
  waiting for transfers between devices  194 us (64%)
  matrix products  30.7 us (10%)
  blocking collectives  26.5 us (9%)
  local copies, waits for them, and re-layouts  20.6 us (7%)
  between operations  15.1 us (5%)
  other arithmetic  14.2 us (5%)
    all_gather x2, waiting for transfers between devices, single_layer(): lax.all_gather(branch_terms, 'tp')  157 us
    reduce_scatter x2, waiting for transfers between devices, single_layer(): lax.psum_scatter(gate_part, 'dp', scatter_dimension=0, tiled=True)  27 us
    unnamed x2, blocking collectives  14.9 us
    all_gather x2, blocking collectives, single_layer(): lax.all_gather(mixed, 'dp', axis=0, tiled=True)  11.6 us
    reduce_scatter x2, waiting for transfers between devices, single_layer(): lax.psum_scatter(input_part, 'dp', scatter_dimension=0, tiled=True)  10 us
    unnamed x44, local copies, waits for them, and re-layouts  8.59 us
  transfers between devices with their start and end apart: 6, of which 5 were waited for; matrix products, arithmetic and copies ran while one was open for 14% of the time, Pallas kernels for 0%

profile of v1, /device:TPU:0, one launch (start us, length us, event | category | flops | bytes accessed | tf_op | source)
XLA Modules:
  0.0 302.1 jit_solution(17038112235495323522)
XLA Ops:
  7.2 0.8 fusion.85
  8.0 2.6 fusion.28
  10.8 2.6 fusion.26
  13.4 0.2 fusion.13
  13.6 8.5 %all-reduce = f32[256]{0:T(256)S(1)} all-reduce(f32[256]{0:T(256)S(1)} %fusion.13), channel_id=5, replica_groups=mesh['grp'=2,'tp'=4,'dp'=4] {'dp'}, use_global_device_ids=true, to_apply=%region_2.4.clone | all-reduce | flops 256 | bytes 2048
  22.2 0.6 fusion.86
  22.8 0.1 slice_reduce_fusion
  22.9 0.1 reshape_squeeze.13
  22.9 0.1 reshape_squeeze.12
  23.0 0.8 slice_bitcast_fusion.1
  23.8 0.9 fusion.84
  24.7 1.6 copy.53
  26.3 1.9 copy.51
  28.3 0.6 gather_fusion.1
  28.9 2.2 gather_fusion
  31.1 0.1 fusion.72
  31.3 1.7 fusion.83
  33.0 0.6 dynamic-slice
  34.3 0.1 fusion.80
  34.3 2.5 copy_bitcast_fusion
  36.9 0.2 exponential_multiply_fusion.1
  37.1 1.0 multiply_convert_fusion.3
  38.1 0.1 copy.43
  38.2 0.8 fusion.50
  39.0 2.8 fusion.5
  41.9 1.7 fusion.48
  43.6 1.8 convolution_subtract_fusion.1
  45.4 0.1 copy.44
  45.5 14.1 %reduce-scatter.7.cloned.1.call-done = f32[64,512]{1,0:T(8,128)} async-done(((f32[256,512]{1,0:T(8,128)}), f32[64,512]{1,0:T(8,128)}) %reduce-scatter.7.cloned.1.call-update) | async-done | bytes 131088 | tf_op jit(solution)/shard_map/reduce_scatter | solution.py:98
  59.6 1.1 fusion.62
  60.7 5.8 %all_gather.18 = bf16[256,512]{1,0:T(8,128)(2,1)S(1)} all-gather(bf16[64,512]{1,0:T(8,128)(2,1)S(1)} %fusion.62), channel_id=1, replica_groups=mesh['grp'=2,'tp'=4,'dp'=4] {'dp'}, dimensions={0}, use_global_device_ids=true | all-gather | bytes 327680 | tf_op jit(solution)/shard_map/all_gather | solution.py:123
  66.5 2.6 fusion.24
  69.2 80.8 %all-gather.5.cloned.1.call-done = f32[1024,1024]{1,0:T(8,128)} async-done(((f32[256,1024]{1,0:T(8,128)}), f32[1024,1024]{1,0:T(8,128)}) %all-gather.5.cloned.1.call-update) | async-done | bytes 4194320 | tf_op jit(solution)/shard_map/all_gather | solution.py:127
  150.0 2.7 reduce_sum.37
  152.7 1.3 fusion.16
  154.0 2.7 fusion.22
  156.8 0.1 reshape_squeeze.15
  156.8 0.1 reshape_squeeze.14
  157.0 0.8 exponential_multiply_fusion
  157.8 6.4 %all-reduce.1 = f32[256]{0:T(256)S(1)} all-reduce(f32[256]{0:T(256)S(1)} %get-tuple-element.13), channel_id=8, replica_groups=mesh['grp'=2,'tp'=4,'dp'=4] {'dp'}, use_global_device_ids=true, to_apply=%region_7.9.clone | all-reduce | flops 256 | bytes 2048
  164.2 0.1 fusion.81
  164.3 2.5 fusion.20
  166.8 0.2 all-gather.7.cloned.1.call-start
  167.0 10.0 %reduce-scatter.9.cloned.1.call-done = f32[64,512]{1,0:T(8,128)} async-done(((f32[256,512]{1,0:T(8,128)}), f32[64,512]{1,0:T(8,128)}) %reduce-scatter.9.cloned.1.call-update) | async-done | bytes 131088 | tf_op jit(solution)/shard_map/reduce_scatter | solution.py:97
  177.0 1.0 multiply_convert_fusion.1
  178.0 0.1 copy.48
  178.2 0.8 fusion.43
  179.0 2.9 fusion.11
  181.9 0.9 copy-done
  182.9 1.7 fusion.41
  184.6 2.5 convolution_subtract_fusion
  187.1 1.1 copy.49
  188.2 12.9 %reduce-scatter.11.cloned.1.call-done = f32[64,512]{1,0:T(8,128)} async-done(((f32[256,512]{1,0:T(8,128)}), f32[64,512]{1,0:T(8,128)}) %reduce-scatter.11.cloned.1.call-update) | async-done | bytes 131088 | tf_op jit(solution)/shard_map/reduce_scatter | solution.py:98
  201.1 1.1 fusion.71
  202.1 5.8 %all_gather.21 = bf16[256,512]{1,0:T(8,128)(2,1)S(1)} all-gather(bf16[64,512]{1,0:T(8,128)(2,1)S(1)} %fusion.71), channel_id=1, replica_groups=mesh['grp'=2,'tp'=4,'dp'=4] {'dp'}, dimensions={0}, use_global_device_ids=true | all-gather | bytes 327680 | tf_op jit(solution)/shard_map/all_gather | solution.py:123
  207.9 2.6 fusion.18
  210.6 0.3 maximum_bitcast_fusion
  210.9 0.9 copy-done.1
  211.8 0.3 maximum_bitcast_fusion.1
  212.1 0.2 pad_maximum_fusion
  212.4 2.5 copy.50
  214.9 76.5 %all-gather.7.cloned.1.call-done = f32[1024,1024]{1,0:T(8,128)} async-done(((f32[256,1024]{1,0:T(8,128)}), f32[1024,1024]{1,0:T(8,128)}) %all-gather.7.cloned.1.call-update) | async-done | bytes 4194320 | tf_op jit(solution)/shard_map/all_gather | solution.py:127
  291.5 2.8 reduce_sum.39
  294.2 1.0 fusion.17
  (56 shorter events, 0.6 us)
Async XLA Ops:
  7.2 3.6 %copy-start.4 = (bf16[256,1024]{1,0:T(8,128)(2,1)S(1)}, bf16[256,1024]{1,0:T(8,128)(2,1)}, u32[]{:S(2)}) copy-start(bf16[256,1024]{1,0:T(8,128)(2,1)} %param.16) | copy-start | bytes 1572868
  7.2 29.9 %reduce-scatter.5.cloned.1.call-start = ((), (), s32[]{:S(2)}) async-start(), calls=%async_computation.4 | async-start | bytes 655360 | tf_op jit(solution)/shard_map/reduce_scatter | solution.py:97
  10.6 11.5 %copy-start.18 = (s32[64]{0:T(128)S(1)}, s32[64]{0:T(128)}, u32[]{:S(2)}) copy-start(s32[64]{0:T(128)} %param.17) | copy-start | bytes 772
  10.6 11.5 %copy-start.17 = (f32[2,32]{1,0:T(2,128)S(1)}, f32[2,32]{1,0:T(2,128)}, u32[]{:S(2)}) copy-start(f32[2,32]{1,0:T(2,128)} %param.25) | copy-start | bytes 772
  10.6 11.5 %copy-start.14 = (f32[2,512]{1,0:T(2,128)S(1)}, f32[2,512]{1,0:T(2,128)}, u32[]{:S(2)}) copy-start(f32[2,512]{1,0:T(2,128)} %param.28) | copy-start | bytes 12292
  10.6 12.1 %copy-start.11 = (f32[2,2048]{1,0:T(2,128)S(1)}, f32[2,2048]{1,0:T(2,128)}, u32[]{:S(2)}) copy-start(f32[2,2048]{1,0:T(2,128)} %param.24) | copy-start | bytes 49156
  10.7 12.1 %copy-start.12 = (f32[2,2048]{1,0:T(2,128)S(1)}, f32[2,2048]{1,0:T(2,128)}, u32[]{:S(2)}) copy-start(f32[2,2048]{1,0:T(2,128)} %param.23) | copy-start | bytes 49156
  10.7 12.3 %copy-start.7 = (f32[2,32,16,128]{3,2,1,0:T(8,128)S(1)}, f32[2,32,16,128]{3,2,1,0:T(8,128)}, u32[]{:S(2)}) copy-start(f32[2,32,16,128]{3,2,1,0:T(8,128)} %param.26) | copy-start | bytes 1572868
  10.7 13.1 %copy-start.8 = (f32[2,32,16,128]{3,2,1,0:T(8,128)S(1)}, f32[2,32,16,128]{3,2,1,0:T(8,128)}, u32[]{:S(2)}) copy-start(f32[2,32,16,128]{3,2,1,0:T(8,128)} %param.27) | copy-start | bytes 1572868
  10.7 48.9 %reduce-scatter.7.cloned.1.call-start = ((), (), s32[]{:S(2)}) async-start(), calls=%async_computation.5 | async-start | bytes 655360 | tf_op jit(solution)/shard_map/reduce_scatter | solution.py:98
  13.4 10.5 %copy-start.5 = (f32[2,32,4096]{2,1,0:T(8,128)S(1)}, f32[2,32,4096]{2,1,0:T(8,128)}, u32[]{:S(2)}) copy-start(f32[2,32,4096]{2,1,0:T(8,128)} %param.29) | copy-start | bytes 3145732
  13.4 136.6 %all-gather.5.cloned.1.call-start = ((), (), s32[]{:S(2)}) async-start(), calls=%async_computation.8 | async-start | bytes 5242880 | tf_op jit(solution)/shard_map/all_gather | solution.py:127
  31.3 1.8 copy-start.19
  41.9 17.8 %copy-start.9 = (f32[64,512]{1,0:T(8,128)S(1)}, f32[64,512]{1,0:T(8,128)}, u32[]{:S(2)}) copy-start(f32[64,512]{1,0:T(8,128)} %reduce-scatter.5.cloned.1.call-done) | copy-start | bytes 393220
  69.1 107.9 %reduce-scatter.9.cloned.1.call-start = ((), (), s32[]{:S(2)}) async-start(), calls=%async_computation.6 | async-start | bytes 655360 | tf_op jit(solution)/shard_map/reduce_scatter | solution.py:97
  154.0 12.8 %copy-start.2 = (bf16[256,1024]{1,0:T(8,128)(2,1)}, bf16[256,1024]{1,0:T(8,128)(2,1)S(1)}, u32[]{:S(2)}) copy-start(bf16[256,1024]{1,0:T(8,128)(2,1)S(1)} %get-tuple-element.14) | copy-start | bytes 1572868
  156.7 21.5 %copy-start.6 = (f32[32,16,128]{2,1,0:T(8,128)S(1)}, f32[32,16,128]{2,1,0:T(8,128)}, u32[]{:S(2)}) copy-start(f32[32,16,128]{2,1,0:T(8,128)} %get-tuple-element.27) | copy-start | bytes 786436
  156.7 44.3 %reduce-scatter.11.cloned.1.call-start = ((), (), s32[]{:S(2)}) async-start(), calls=%async_computation.7 | async-start | bytes 655360 | tf_op jit(solution)/shard_map/reduce_scatter | solution.py:98
  164.3 12.8 %copy-start.15 = (f32[64]{0:T(128)}, f32[64]{0:T(128)S(1)}, u32[]{:S(2)}) copy-start(f32[64]{0:T(128)S(1)} %fusion.81) | copy-start | bytes 772
  166.8 124.7 %all-gather.7.cloned.1.call-start = ((), (), s32[]{:S(2)}) async-start(), calls=%async_computation.9 | async-start | bytes 5242880 | tf_op jit(solution)/shard_map/all_gather | solution.py:127
  181.9 1.0 copy-start
  181.9 19.2 %copy-start.10 = (f32[64,512]{1,0:T(8,128)S(1)}, f32[64,512]{1,0:T(8,128)}, u32[]{:S(2)}) copy-start(f32[64,512]{1,0:T(8,128)} %reduce-scatter.9.cloned.1.call-done) | copy-start | bytes 393220
  181.9 19.2 %copy-start.13 = (f32[1,512]{1,0:T(1,128)S(1)}, f32[1,512]{1,0:T(1,128)}, u32[]{:S(2)}) copy-start(f32[1,512]{1,0:T(1,128)} %get-tuple-element.39) | copy-start | bytes 6148
  181.9 19.2 %copy-start.16 = (f32[64]{0:T(128)S(1)}, f32[64]{0:T(128)}, u32[]{:S(2)}) copy-start(f32[64]{0:T(128)} %copy-done.15) | copy-start | bytes 772
  210.6 1.2 copy-start.1
  291.5 2.8 copy-start.3
Sparse Core Ops, SparseCore 0:
  11.0 24.3 reduce-scatter.4
  37.9 21.6 reduce-scatter.6
  69.2 80.7 all-gather.4
  156.8 20.1 reduce-scatter.8
  179.4 21.6 reduce-scatter.10
  210.7 80.7 all-gather.6
